TPU v7x, 32 devices: a whole 2x2x4 slice. The times are simulated.
32 devices in a mesh: sp: 8 (over z, y), tp: 4 (over x, core).
Axes of the slice: x: 2, y: 2, z: 4, core: 2. Of those that a mesh axis runs over, the one named last changes fastest.
Arguments:
- tokens: bfloat16 [4096, 2048], P(('sp', 'tp')), may hold values from -6 to 6
- norm_gain: bfloat16 [2048], replicated, may hold values from 0.099609375 to 1.8984375
- proj_x: bfloat16 [2048, 2048], P('sp', 'tp'), may hold values from -0.125 to 0.125
- gate_projection: bfloat16 [2048, 2048], P('sp', 'tp'), may hold values from -0.125 to 0.125
- conv_taps: bfloat16 [4, 2048], P(None, 'tp'), may hold values from -3 to 3
- gate_recur: bfloat16 [8, 256, 256], P('tp'), may hold values from -0.375 to 0.375
- gate_input: bfloat16 [8, 256, 256], P('tp'), may hold values from -0.375 to 0.375
- decay_param: float32 [2048], P('tp'), may hold values from 4 to 25
- decay_shift: float32 [8, 4096], P('tp', 'sp'), may hold values from -1.3 to 0, as said below
- proj_out: bfloat16 [2048, 2048], P('tp', 'sp'), may hold values from -0.125 to 0.125
Outputs:
- mixed_out: bfloat16 [4096, 2048], P(('sp', 'tp'))
Inputs may be any that keep to these rules, and one draw needn't show every extreme that they name: `decay_shift`: added log-decays, never positive.
All inputs are finite; a program needn't handle non-finite values.
Results may differ from a plain program's by a relative error of at most 0.015.
Values may be sent and summed in bfloat16 or wider, within the bound.
A program may use at most 128 MiB of HBM per device.

v0:
```python
import jax
import jax.numpy as jnp
from jax import lax
from jax.sharding import PartitionSpec as P

HEAD = 256
CONV = 4


def shifted(block, axis, distance):
    devices = range(lax.axis_size(axis))
    route = [(i - distance, i) for i in devices if i - distance in devices]
    return lax.ppermute(block, axis, route)


def carried_in(array, axis, combine, identity):
    size, index = (lax.axis_size(axis), lax.axis_index(axis))
    everything = jax.tree.map(lambda part: lax.all_gather(part, axis), array)
    start = jax.tree.map(
        lambda part, zero: jnp.broadcast_to(jnp.asarray(zero, part.dtype), part.shape),
        array,
        identity,
    )

    def turn(k, before):
        reached = k < index
        new = combine(before, jax.tree.map(lambda part: part[k], everything))
        return jax.tree.map(lambda a, b: jnp.where(reached, a, b), new, before)

    return lax.fori_loop(0, size, turn, start)


def rms_norm(values, norm_gain):
    floats = values.astype(jnp.float32)
    scaled = floats * lax.rsqrt(jnp.mean(floats * floats, axis=-1, keepdims=True) + 1e-06)
    return (scaled * norm_gain.astype(jnp.float32)).astype(jnp.bfloat16)


def combine_pair(earlier, later):
    return (earlier[0] * later[0], later[0] * earlier[1] + later[1])


def on_device(
    tokens,
    norm_gain,
    proj_x,
    gate_projection,
    conv_taps,
    gate_recur,
    gate_input,
    decay_param,
    decay_shift,
    proj_out,
):
    normed = rms_norm(tokens, norm_gain)
    full_x, full_gate = (
        lax.all_gather(proj_x, "sp", axis=0, tiled=True),
        lax.all_gather(gate_projection, "sp", axis=0, tiled=True),
    )
    local_width = proj_x.shape[1]
    piece = lax.all_gather(normed, "tp", axis=0, tiled=True)
    branch_piece = jnp.dot(piece, full_x, preferred_element_type=jnp.float32).astype(jnp.bfloat16)
    gating_piece = jnp.dot(piece, full_gate, preferred_element_type=jnp.float32).astype(
        jnp.bfloat16
    )
    joined = jnp.concatenate([branch_piece, gating_piece], axis=1)
    branch = joined[:, :local_width]
    gating = joined[:, local_width:]
    row_count = branch.shape[0]
    tail_rows = shifted(branch[row_count - CONV + 1 :], "sp", 1)
    extended = jnp.concatenate([tail_rows, branch], axis=0)
    conv_sum = jnp.zeros((row_count, local_width), jnp.float32)
    for tap_index in range(CONV):
        conv_sum = conv_sum + extended[tap_index : tap_index + row_count].astype(
            jnp.float32
        ) * conv_taps[tap_index].astype(jnp.float32)
    conved = conv_sum.astype(jnp.bfloat16)
    head_count = gate_recur.shape[0]
    grouped = conved.reshape(row_count, head_count, HEAD)
    recur = jax.nn.sigmoid(
        jnp.einsum("thi,hij->thj", grouped, gate_recur, preferred_element_type=jnp.float32)
    )
    inlet = jax.nn.sigmoid(
        jnp.einsum("thi,hij->thj", grouped, gate_input, preferred_element_type=jnp.float32)
    )
    decay_rate = jax.nn.softplus(-decay_param).reshape(head_count, HEAD)
    log_decay = (-8.0 * recur * decay_rate[None] + jnp.transpose(decay_shift)[:, :, None]).reshape(
        row_count, local_width
    )
    decay = jnp.exp(log_decay)
    drive = (
        jnp.sqrt(-jnp.expm1(2.0 * log_decay))
        * inlet.reshape(row_count, local_width)
        * conved.astype(jnp.float32)
    )
    identity = (jnp.ones((local_width,), jnp.float32), jnp.zeros((local_width,), jnp.float32))
    cumulative, local_state = lax.associative_scan(combine_pair, (decay, drive), axis=0)
    carried = carried_in(
        (cumulative[row_count - 1], local_state[row_count - 1]), "sp", combine_pair, identity
    )
    states = local_state + cumulative * carried[1][None, :]
    mixed = (states * jax.nn.gelu(gating.astype(jnp.float32))).astype(jnp.bfloat16)
    out_cols = lax.all_gather(proj_out, "sp", axis=1, tiled=True)
    return lax.psum_scatter(
        jnp.dot(mixed, out_cols, preferred_element_type=jnp.float32).astype(jnp.bfloat16),
        "tp",
        scatter_dimension=0,
        tiled=True,
    )


def solution(mesh):
    in_specs = (
        P(("sp", "tp"), None),
        P(),
        P("sp", "tp"),
        P("sp", "tp"),
        P(None, "tp"),
        P("tp", None, None),
        P("tp", None, None),
        P("tp"),
        P("tp", "sp"),
        P("tp", "sp"),
    )
    out_specs = P(("sp", "tp"), None)
    return jax.shard_map(
        on_device, mesh=mesh, in_specs=in_specs, out_specs=out_specs, check_vma=False
    )
```

profile of v0, /device:TPU:0, one launch (start us, length us, event | category | flops | bytes accessed | tf_op | source)
XLA Modules:
  0.0 287.4 jit_solution(4033228351637639462)
XLA Ops:
  6.5 1.3 fusion.11
  7.8 0.7 convert_element_type.51
  8.5 2.0 fusion.13
  10.6 0.7 all-gather.9.cloned.1.call-update
  11.4 0.7 all-gather.11.cloned.1.call-update
  12.1 0.5 all-gather.13.cloned.1.call-update
  12.7 23.3 %all-gather.7.cloned.1.call-done = bf16[512,2048]{1,0:T(8,128)(2,1)} async-done(((bf16[128,2048]{1,0:T(8,128)(2,1)}), bf16[512,2048]{1,0:T(8,128)(2,1)}) %all-gather.7.cloned.1.call-update) | async-done | bytes 2097168 | tf_op jit(solution)/shard_map/all_gather | solution.py:61
  36.0 51.2 %all-gather.9.cloned.1.call-done = bf16[2048,512]{1,0:T(8,128)(2,1)} async-done(((bf16[256,512]{1,0:T(8,128)(2,1)}), bf16[2048,512]{1,0:T(8,128)(2,1)}) %all-gather.9.cloned.1.call-update) | async-done | bytes 2097168 | tf_op jit(solution)/shard_map/all_gather | solution.py:57
  87.3 3.5 %convolution_convert_fusion.2 = bf16[512,512]{1,0:T(8,128)(2,1)S(1)} fusion(bf16[512,2048]{1,0:T(8,128)(2,1)} %all-gather.7.cloned.1.call-done, bf16[2048,512]{1,0:T(8,128)(2,1)} %all-gather.9.cloned.1.call-done), kind=kOutput, calls=%fused_computation.24 | convolution fusion | flops 1074003968 | bytes 4718592 | tf_op jit(solution)/shard_map/dot_general | solution.py:62
  90.7 2.5 collective-permute-start
  93.3 1.2 collective-permute-done
  94.5 0.5 add_convert_fusion
  95.1 0.6 fusion.49
  95.7 0.1 copy-done.2
  95.8 0.4 copy-done.11
  96.2 1.9 fusion.4
  98.1 1.6 copy.31
  99.7 1.2 convert_multiply_fusion.5
  100.9 2.3 slice.367
  103.2 2.1 slice.305
  105.3 2.1 slice.304
  107.3 0.2 slice_reduce_fusion
  107.5 19.5 %slice.303 = f32[256,512]{0,1:T(8,128)S(1)} slice(f32[512,512]{0,1:T(8,128)S(1)} %bitcast.49), slice={[1:512:2], [0:512:1]} | slice | bytes 1048576 | tf_op jit(solution)/shard_map/slice | solution.py:97
  127.0 19.4 %slice.302 = f32[255,512]{0,1:T(8,128)S(1)} slice(f32[512,512]{0,1:T(8,128)S(1)} %bitcast.50), slice={[2:512:2], [0:512:1]} | slice | bytes 1044480 | tf_op jit(solution)/shard_map/slice | solution.py:97
  146.4 19.5 %slice.307 = f32[256,512]{0,1:T(8,128)S(1)} slice(f32[512,512]{0,1:T(8,128)S(1)} %bitcast.51), slice={[0:511:2], [0:512:1]} | slice | bytes 1048576 | tf_op jit(solution)/shard_map/slice | solution.py:97
  165.9 1.0 copy.36
  166.9 0.2 copy.37
  167.1 0.1 copy-done.4
  167.3 1.3 multiply_add_fusion
  168.5 0.3 slice.365
  168.9 0.3 slice.311
  169.2 0.3 slice.310
  169.6 0.3 slice.313
  169.9 0.3 slice.309
  170.2 0.3 slice.308
  170.6 0.1 multiply_add_fusion.1
  170.7 0.2 slice.363
  170.9 0.1 slice.317
  171.0 0.1 slice.316
  171.1 0.1 slice.319
  171.2 0.1 slice.315
  171.3 0.4 slice.314
  172.7 1.0 copy.35
  174.9 0.2 fusion.33
  175.1 0.1 pad.142
  175.2 0.1 pad.124
  175.3 0.1 pad.125
  175.4 0.1 pad.143
  175.5 0.1 add.303
  175.6 0.1 add.293
  175.7 0.9 copy-done.5
  176.5 0.2 copy-done.6
  176.7 1.2 fusion.25
  177.9 2.9 pad.144
  180.8 2.7 pad.126
  183.6 2.7 pad.127
  186.3 0.7 add_bitcast_fusion
  187.0 27.3 %all-gather.1 = f32[8,1,512]{2,1,0:T(1,128)S(1)} all-gather(f32[1,1,512]{2,1,0:T(1,128)S(1)} %add_bitcast_fusion), channel_id=1, replica_groups=mesh['sp'=8,'tp'=4] {'sp'}, dimensions={0}, use_global_device_ids=true | all-gather | bytes 18432 | tf_op jit(solution)/shard_map/all_gather | solution.py:18
  214.3 2.8 pad.145
  217.1 0.7 add_bitcast_fusion.1
  217.8 26.1 %all-gather = f32[8,1,512]{2,1,0:T(1,128)S(1)} all-gather(f32[1,1,512]{2,1,0:T(1,128)S(1)} %add_bitcast_fusion.1), channel_id=1, replica_groups=mesh['sp'=8,'tp'=4] {'sp'}, dimensions={0}, use_global_device_ids=true | all-gather | bytes 18432 | tf_op jit(solution)/shard_map/all_gather | solution.py:18
  243.9 0.4 while.14
  244.4 7.9 %convolution_convert_fusion = bf16[512,2048]{1,0:T(8,128)(2,1)} fusion(bf16[512,2048]{1,0:T(8,128)(2,1)} %all-gather.13.cloned.1.call-done, bf16[512,2048]{1,0:T(8,128)(2,1)} %all-gather.7.cloned.1.call-done, bf16[2048,512]{1,0:T(8,128)(2,1)} %all-gather.11.cloned.1.call-done, f32[512,512]{1,0:T(8,128)S(1)} %copy-done.8, f32[512,512]{1,0:T(8,128)} %pad.145, ...), kind=kOutput, calls=%fused_computation.3 | convolution fusion | flops 2152726528 | bytes 12584960 | tf_op jit(solution)/shard_map/dot_general | solution.py:105
  252.3 28.5 %reduce-scatter.2.cloned.1.call-done = bf16[128,2048]{1,0:T(8,128)(2,1)} async-done(((bf16[512,2048]{1,0:T(8,128)(2,1)}), bf16[128,2048]{1,0:T(8,128)(2,1)}) %reduce-scatter.2.cloned.1.call-update) | async-done | bytes 524304 | tf_op jit(solution)/shard_map/reduce_scatter | solution.py:104
  (162 shorter events, 2.3 us)
Async XLA Ops:
  6.5 88.5 %copy-start = (bf16[2,256,256]{2,1,0:T(8,128)(2,1)S(1)}, bf16[2,256,256]{2,1,0:T(8,128)(2,1)}, u32[]{:S(2)}) copy-start(bf16[2,256,256]{2,1,0:T(8,128)(2,1)} %param.17) | copy-start | bytes 786436
  6.5 6.1 %copy-start.9 = (bf16[4,512]{1,0:T(4,128)(2,1)S(1)}, bf16[4,512]{1,0:T(4,128)(2,1)}, u32[]{:S(2)}) copy-start(bf16[4,512]{1,0:T(4,128)(2,1)} %param.16) | copy-start | bytes 12292
  6.5 29.5 %all-gather.7.cloned.1.call-start = ((), (), s32[]{:S(2)}) async-start(), calls=%async_computation.1 | async-start | bytes 2621440 | tf_op jit(solution)/shard_map/all_gather | solution.py:61
  10.6 76.7 %all-gather.9.cloned.1.call-start = ((), (), s32[]{:S(2)}) async-start(), calls=%async_computation.2 | async-start | bytes 2359296 | tf_op jit(solution)/shard_map/all_gather | solution.py:57
  11.3 233.0 %all-gather.11.cloned.1.call-start = ((), (), s32[]{:S(2)}) async-start(), calls=%async_computation.3 | async-start | bytes 2359296 | tf_op jit(solution)/shard_map/all_gather | solution.py:58
  12.1 232.3 %all-gather.13.cloned.1.call-start = ((), (), s32[]{:S(2)}) async-start(), calls=%async_computation.4 | async-start | bytes 2359296 | tf_op jit(solution)/shard_map/all_gather | solution.py:103
  12.6 268.2 %reduce-scatter.2.cloned.1.call-start = ((), (), s32[]{:S(2)}) async-start(), calls=%async_computation.5 | async-start | bytes 2621440 | tf_op jit(solution)/shard_map/reduce_scatter | solution.py:104
  12.7 80.5 %copy-start.10 = (f32[512]{0:T(512)S(1)}, f32[512]{0:T(512)}, u32[]{:S(2)}) copy-start(f32[512]{0:T(512)} %param.19) | copy-start | bytes 6148
  12.7 82.3 %copy-start.12 = (f32[2,512]{1,0:T(2,128)S(1)}, f32[2,512]{1,0:T(2,128)}, u32[]{:S(2)}) copy-start(f32[2,512]{1,0:T(2,128)} %param.20) | copy-start | bytes 12292
  90.7 3.8 %collective-permute-start = (bf16[3,512]{1,0:T(4,128)(2,1)S(1)}, bf16[3,512]{1,0:T(4,128)(2,1)S(1)}, u32[]{:S(2)}, u32[]{:S(2)}) collective-permute-start(bf16[3,512]{1,0:T(4,128)(2,1)S(1)} %slice.388), channel_id=1, source_target_pairs={{0,4},{4,8},{8,12},{12,16},{16,20},{20,24},{24,28},{1,5},{5,9},{9,... | collective-permute-start | bytes 9224 | tf_op jit(solution)/shard_map/ppermute | solution.py:13
  95.0 0.8 copy-start.2
  95.1 1.1 copy-start.11
  100.9 26.1 %copy-start.1 = (f32[512,512]{1,0:T(8,128)}, f32[512,512]{1,0:T(8,128)S(1)}, u32[]{:S(2)}) copy-start(f32[512,512]{1,0:T(8,128)S(1)} %convert_multiply_fusion.5) | copy-start | bytes 3145732
  165.9 1.3 copy-start.3
  165.9 1.4 copy-start.4
  175.5 1.1 copy-start.5
  175.5 1.2 copy-start.6
  177.8 2.9 %slice-start = ((f32[512,512]{1,0:T(8,128)}), f32[1,512]{1,0:T(1,128)S(1)}, s32[]{:S(2)}) async-start(f32[512,512]{1,0:T(8,128)} %copy-done.1), calls=%async_computation.6 | async-start | bytes 4096 | tf_op jit(solution)/shard_map/slice | solution.py:97
  177.8 2.9 %copy-start.7 = (f32[255,512]{1,0:T(8,128)S(1)}, f32[255,512]{1,0:T(8,128)}, u32[]{:S(2)}) copy-start(f32[255,512]{1,0:T(8,128)} %get-tuple-element.130) | copy-start | bytes 1566724
  180.8 36.3 %copy-start.8 = (f32[512,512]{1,0:T(8,128)S(1)}, f32[512,512]{1,0:T(8,128)}, u32[]{:S(2)}) copy-start(f32[512,512]{1,0:T(8,128)} %pad.144) | copy-start | bytes 3145732
Sparse Core Ops, SparseCore 0:
  10.7 25.2 all-gather.6
  38.1 49.0 all-gather.8
  89.4 47.6 all-gather.10
  139.0 48.8 all-gather.12
  252.4 28.3 reduce-scatter.1
where the time goes:
time: 288 us; the launch traced here: 287 us
  waiting for transfers between devices  106 us (37%)
  local copies, waits for them, and re-layouts  85.9 us (30%)
  blocking collectives  53.4 us (19%)
  between operations  14.1 us (5%)
  matrix products  13.9 us (5%)
  other arithmetic  10.9 us (4%)
    slice x61, local copies, waits for them, and re-layouts, on_device(): lax.associative_scan(combine_pair, (decay, drive), axis=0)  68.6 us
    all_gather x2, blocking collectives, carried_in(): everything = jax.tree.map(lambda part: lax.all_gather(part, axis), array)  53.4 us
    all_gather x1, waiting for transfers between devices, on_device(): lax.all_gather(proj_x, 'sp', axis=0, tiled=True)  51.2 us
    reduce_scatter x1, waiting for transfers between devices, on_device(): lax.psum_scatter(jnp.dot(mixed, out_cols, preferred_element_type=jnp.floa...  28.5 us
    all_gather x1, waiting for transfers between devices, on_device(): piece = lax.all_gather(normed, 'tp', axis=0, tiled=True)  23.3 us
    pad x32, local copies, waits for them, and re-layouts, on_device(): lax.associative_scan(combine_pair, (decay, drive), axis=0)  11.7 us
    dot_general x1, matrix products, on_device(): jnp.dot(mixed, out_cols, preferred_element_type=jnp.float32)  7.88 us
  transfers between devices with their start and end apart: 6, of which 4 were waited for; matrix products, arithmetic and copies ran while one was open for 34% of the time, Pallas kernels for 0%

commit v1 on v0

--- a/solution.py
+++ b/solution.py
@@ -54,7 +54,9 @@
 ):
     normed = rms_norm(tokens, norm_gain)
     full_x, full_gate = (
-        lax.all_gather(proj_x, "sp", axis=0, tiled=True),
+        jnp.concatenate(
+            lax.all_to_all(jnp.stack([proj_x] * lax.axis_size("sp")), "sp", 0, 0), axis=0
+        ),
         lax.all_gather(gate_projection, "sp", axis=0, tiled=True),
     )
     local_width = proj_x.shape[1]

time: 288 us -> 278 us (0.965)
  waiting for transfers between devices: 106 us -> 87.2 us
  starting transfers between devices: 2.62 us -> 10.9 us
    all_gather x1 -> x0, waiting for transfers between devices: 51.2 us -> none  [on_device(): lax.all_gather(proj_x, 'sp', axis=0, tiled=True)]
    all_to_all x0 -> x1, waiting for transfers between devices: none -> 41 us  [on_device(): lax.all_to_all(jnp.stack([proj_x] * lax.axis_size('sp')), 'sp', 0, 0)]
    all_gather x1, waiting for transfers between devices: 23.3 us -> 14.8 us  [on_device(): piece = lax.all_gather(normed, 'tp', axis=0, tiled=True)]
    all_to_all x0 -> x1, starting transfers between devices: none -> 7.44 us  [on_device(): lax.all_to_all(jnp.stack([proj_x] * lax.axis_size('sp')), 'sp', 0, 0)]
  transfers between devices with their start and end apart: 6 -> 6, of which waited for: 4 -> 4; matrix products, arithmetic and copies ran while one was open for 34% -> 35% of each run, Pallas kernels for 0% -> 0%
where the time goes in v1:
time: 278 us
  local copies, waits for them, and re-layouts  87.5 us (31%)
  waiting for transfers between devices  87.2 us (31%)
  blocking collectives  53.6 us (19%)
  between operations  14.1 us (5%)
  matrix products  13.3 us (5%)
  starting transfers between devices  10.9 us (4%)
  other arithmetic  10.9 us (4%)
    slice x61, local copies, waits for them, and re-layouts, on_device(): lax.associative_scan(combine_pair, (decay, drive), axis=0)  68.6 us
    all_gather x2, blocking collectives, carried_in(): everything = jax.tree.map(lambda part: lax.all_gather(part, axis), array)  53.6 us
    all_to_all x1, waiting for transfers between devices, on_device(): lax.all_to_all(jnp.stack([proj_x] * lax.axis_size('sp')), 'sp', 0, 0)  41 us
    reduce_scatter x1, waiting for transfers between devices, on_device(): lax.psum_scatter(jnp.dot(mixed, out_cols, preferred_element_type=jnp.floa...  28.6 us
    all_gather x1, waiting for transfers between devices, on_device(): piece = lax.all_gather(normed, 'tp', axis=0, tiled=True)  14.8 us
    pad x32, local copies, waits for them, and re-layouts, on_device(): lax.associative_scan(combine_pair, (decay, drive), axis=0)  11.7 us
    dot_general x1, matrix products, on_device(): jnp.dot(mixed, out_cols, preferred_element_type=jnp.float32)  7.88 us
    all_to_all x1, starting transfers between devices, on_device(): lax.all_to_all(jnp.stack([proj_x] * lax.axis_size('sp')), 'sp', 0, 0)  7.44 us
  transfers between devices with their start and end apart: 6, of which 4 were waited for; matrix products, arithmetic and copies ran while one was open for 35% of the time, Pallas kernels for 0%

profile of v1, /device:TPU:0, one launch (start us, length us, event | category | flops | bytes accessed | tf_op | source)
XLA Modules:
  0.0 277.6 jit_solution(5921983017120593081)
XLA Ops:
  6.5 1.3 fusion.11
  7.8 0.7 convert_element_type.51
  8.5 2.0 fusion.13
  10.6 0.7 all-gather.8.cloned.1.call-update
  11.3 1.6 stack.2
  12.9 7.4 %all-to-all-start = ((bf16[8,256,512]{2,1,0:T(8,128)(2,1)}), bf16[8,256,512]{2,1,0:T(8,128)(2,1)S(1)}, u32[]{:S(2)}, u32[]{:S(2)}) async-start(bf16[8,256,512]{2,1,0:T(8,128)(2,1)} %stack.2), calls=%async_computation | async-start | bytes 4194304 | tf_op jit(solution)/shard_map/all_to_all | solution.py:58
  20.4 0.7 all-gather.10.cloned.1.call-update
  21.2 14.8 %all-gather.6.cloned.1.call-done = bf16[512,2048]{1,0:T(8,128)(2,1)} async-done(((bf16[128,2048]{1,0:T(8,128)(2,1)}), bf16[512,2048]{1,0:T(8,128)(2,1)}) %all-gather.6.cloned.1.call-update) | async-done | bytes 2097168 | tf_op jit(solution)/shard_map/all_gather | solution.py:63
  36.0 41.0 %all-to-all-done = bf16[8,256,512]{2,1,0:T(8,128)(2,1)S(1)} async-done(((bf16[8,256,512]{2,1,0:T(8,128)(2,1)}), bf16[8,256,512]{2,1,0:T(8,128)(2,1)S(1)}, u32[]{:S(2)}, u32[]{:S(2)}) %all-to-all-start) | async-done | bytes 2097184 | tf_op jit(solution)/shard_map/all_to_all | solution.py:58
  77.1 2.8 %convolution_convert_fusion.2 = bf16[512,512]{1,0:T(8,128)(2,1)S(1)} fusion(bf16[512,2048]{1,0:T(8,128)(2,1)} %all-gather.6.cloned.1.call-done, bf16[2048,512]{1,0:T(8,128)(2,1)S(1)} %bitcast.55), kind=kOutput, calls=%fused_computation.24 | convolution fusion | flops 1074003968 | bytes 4718592 | tf_op jit(solution)/shard_map/dot_general | solution.py:64
  79.9 3.4 %collective-permute-start = (bf16[3,512]{1,0:T(4,128)(2,1)S(1)}, bf16[3,512]{1,0:T(4,128)(2,1)S(1)}, u32[]{:S(2)}, u32[]{:S(2)}) collective-permute-start(bf16[3,512]{1,0:T(4,128)(2,1)S(1)} %slice.388), channel_id=1, source_target_pairs={{0,4},{4,8},{8,12},{12,16},{16,20},{20,24},{24,28},{1,5},{5,9},{9,... | collective-permute-start | bytes 9224 | tf_op jit(solution)/shard_map/ppermute | solution.py:13
  83.4 1.3 collective-permute-done
  84.6 0.5 add_convert_fusion
  85.2 0.6 fusion.49
  85.8 0.1 copy-done.2
  85.9 0.4 copy-done.12
  86.3 1.9 fusion.4
  88.2 1.6 copy.31
  89.8 1.2 convert_multiply_fusion.5
  91.0 2.3 slice.367
  93.3 2.1 slice.305
  95.4 2.1 slice.304
  97.5 0.2 slice_reduce_fusion
  97.6 19.5 %slice.303 = f32[256,512]{0,1:T(8,128)S(1)} slice(f32[512,512]{0,1:T(8,128)S(1)} %bitcast.50), slice={[1:512:2], [0:512:1]} | slice | bytes 1048576 | tf_op jit(solution)/shard_map/slice | solution.py:99
  117.1 19.4 %slice.302 = f32[255,512]{0,1:T(8,128)S(1)} slice(f32[512,512]{0,1:T(8,128)S(1)} %bitcast.51), slice={[2:512:2], [0:512:1]} | slice | bytes 1044480 | tf_op jit(solution)/shard_map/slice | solution.py:99
  136.5 19.5 %slice.307 = f32[256,512]{0,1:T(8,128)S(1)} slice(f32[512,512]{0,1:T(8,128)S(1)} %bitcast.52), slice={[0:511:2], [0:512:1]} | slice | bytes 1048576 | tf_op jit(solution)/shard_map/slice | solution.py:99
  156.0 1.0 copy.36
  157.0 0.2 copy.37
  157.2 0.1 copy-done.4
  157.4 1.3 multiply_add_fusion
  158.6 0.3 slice.365
  159.0 0.3 slice.311
  159.3 0.3 slice.310
  159.6 0.3 slice.313
  160.0 0.3 slice.309
  160.3 0.3 slice.308
  160.6 0.1 multiply_add_fusion.1
  160.8 0.2 slice.363
  161.0 0.1 slice.317
  161.1 0.1 slice.316
  161.2 0.1 slice.319
  161.3 0.1 slice.315
  161.4 0.4 slice.314
  162.8 1.0 copy.35
  165.0 0.2 fusion.33
  165.2 0.1 pad.142
  165.3 0.1 pad.124
  165.4 0.1 pad.125
  165.6 0.1 add.303
  165.7 0.1 add.293
  165.8 0.8 copy-done.5
  166.6 0.2 copy-done.6
  166.8 1.2 fusion.25
  168.0 2.9 %pad.144 = f32[512,512]{1,0:T(8,128)} pad(f32[256,512]{1,0:T(8,128)S(1)} %pad_maximum_fusion.2, f32[]{:T(128)} %constant.42.clone.1), padding=0_1_1x0_0_0 | pad | bytes 1572868 | tf_op jit(solution)/shard_map/pad | solution.py:99
  170.9 2.7 pad.126
  173.6 2.7 pad.127
  176.3 0.7 add_bitcast_fusion
  177.1 27.5 %all-gather.1 = f32[8,1,512]{2,1,0:T(1,128)S(1)} all-gather(f32[1,1,512]{2,1,0:T(1,128)S(1)} %add_bitcast_fusion), channel_id=1, replica_groups=mesh['sp'=8,'tp'=4] {'sp'}, dimensions={0}, use_global_device_ids=true | all-gather | bytes 18432 | tf_op jit(solution)/shard_map/all_gather | solution.py:18
  204.5 2.8 pad.145
  207.3 0.7 add_bitcast_fusion.1
  208.0 26.1 %all-gather = f32[8,1,512]{2,1,0:T(1,128)S(1)} all-gather(f32[1,1,512]{2,1,0:T(1,128)S(1)} %add_bitcast_fusion.1), channel_id=1, replica_groups=mesh['sp'=8,'tp'=4] {'sp'}, dimensions={0}, use_global_device_ids=true | all-gather | bytes 18432 | tf_op jit(solution)/shard_map/all_gather | solution.py:18
  234.1 0.4 while.14
  234.6 7.9 %convolution_convert_fusion = bf16[512,2048]{1,0:T(8,128)(2,1)} fusion(bf16[512,2048]{1,0:T(8,128)(2,1)} %all-gather.10.cloned.1.call-done, bf16[512,2048]{1,0:T(8,128)(2,1)} %all-gather.6.cloned.1.call-done, bf16[2048,512]{1,0:T(8,128)(2,1)} %all-gather.8.cloned.1.call-done, f32[512,512]{1,0:T(8,128)S(1)} %copy-done.8, f32[512,512]{1,0:T(8,128)} %pad.145, ...), kind=kOutput, calls=%fused_computation.3 | convolution fusion | flops 2152726528 | bytes 12584960 | tf_op jit(solution)/shard_map/dot_general | solution.py:107
  242.5 28.6 %reduce-scatter.2.cloned.1.call-done = bf16[128,2048]{1,0:T(8,128)(2,1)} async-done(((bf16[512,2048]{1,0:T(8,128)(2,1)}), bf16[128,2048]{1,0:T(8,128)(2,1)}) %reduce-scatter.2.cloned.1.call-update) | async-done | bytes 524304 | tf_op jit(solution)/shard_map/reduce_scatter | solution.py:106
  (164 shorter events, 2.4 us)
Async XLA Ops:
  6.5 78.6 %copy-start = (bf16[2,256,256]{2,1,0:T(8,128)(2,1)S(1)}, bf16[2,256,256]{2,1,0:T(8,128)(2,1)}, u32[]{:S(2)}) copy-start(bf16[2,256,256]{2,1,0:T(8,128)(2,1)} %param.17) | copy-start | bytes 786436
  6.5 4.8 %copy-start.9 = (bf16[256,512]{1,0:T(8,128)(2,1)S(1)}, bf16[256,512]{1,0:T(8,128)(2,1)}, u32[]{:S(2)}) copy-start(bf16[256,512]{1,0:T(8,128)(2,1)} %param.14) | copy-start | bytes 786436
  6.5 29.5 %all-gather.6.cloned.1.call-start = ((), (), s32[]{:S(2)}) async-start(), calls=%async_computation.2 | async-start | bytes 2621440 | tf_op jit(solution)/shard_map/all_gather | solution.py:63
  10.6 224.0 %all-gather.8.cloned.1.call-start = ((), (), s32[]{:S(2)}) async-start(), calls=%async_computation.3 | async-start | bytes 2359296 | tf_op jit(solution)/shard_map/all_gather | solution.py:60
  12.9 8.2 %copy-start.10 = (bf16[4,512]{1,0:T(4,128)(2,1)S(1)}, bf16[4,512]{1,0:T(4,128)(2,1)}, u32[]{:S(2)}) copy-start(bf16[4,512]{1,0:T(4,128)(2,1)} %param.16) | copy-start | bytes 12292
  12.9 64.1 %all-to-all-start = ((bf16[8,256,512]{2,1,0:T(8,128)(2,1)}), bf16[8,256,512]{2,1,0:T(8,128)(2,1)S(1)}, u32[]{:S(2)}, u32[]{:S(2)}) async-start(bf16[8,256,512]{2,1,0:T(8,128)(2,1)} %stack.2), calls=%async_computation | async-start | bytes 4194304 | tf_op jit(solution)/shard_map/all_to_all | solution.py:58
  20.4 214.3 %all-gather.10.cloned.1.call-start = ((), (), s32[]{:S(2)}) async-start(), calls=%async_computation.4 | async-start | bytes 2359296 | tf_op jit(solution)/shard_map/all_gather | solution.py:105
  21.1 250.0 %reduce-scatter.2.cloned.1.call-start = ((), (), s32[]{:S(2)}) async-start(), calls=%async_computation.5 | async-start | bytes 2621440 | tf_op jit(solution)/shard_map/reduce_scatter | solution.py:106
  77.1 6.3 %copy-start.11 = (f32[512]{0:T(512)S(1)}, f32[512]{0:T(512)}, u32[]{:S(2)}) copy-start(f32[512]{0:T(512)} %param.19) | copy-start | bytes 6148
  77.1 8.1 %copy-start.13 = (f32[2,512]{1,0:T(2,128)S(1)}, f32[2,512]{1,0:T(2,128)}, u32[]{:S(2)}) copy-start(f32[2,512]{1,0:T(2,128)} %param.20) | copy-start | bytes 12292
  79.9 4.7 %collective-permute-start = (bf16[3,512]{1,0:T(4,128)(2,1)S(1)}, bf16[3,512]{1,0:T(4,128)(2,1)S(1)}, u32[]{:S(2)}, u32[]{:S(2)}) collective-permute-start(bf16[3,512]{1,0:T(4,128)(2,1)S(1)} %slice.388), channel_id=1, source_target_pairs={{0,4},{4,8},{8,12},{12,16},{16,20},{20,24},{24,28},{1,5},{5,9},{9,... | collective-permute-start | bytes 9224 | tf_op jit(solution)/shard_map/ppermute | solution.py:13
  85.1 0.8 copy-start.2
  85.2 1.1 copy-start.12
  91.0 26.1 %copy-start.1 = (f32[512,512]{1,0:T(8,128)}, f32[512,512]{1,0:T(8,128)S(1)}, u32[]{:S(2)}) copy-start(f32[512,512]{1,0:T(8,128)S(1)} %convert_multiply_fusion.5) | copy-start | bytes 3145732
  156.0 1.3 copy-start.3
  156.0 1.4 copy-start.4
  165.6 1.0 copy-start.5
  165.6 1.2 copy-start.6
  167.9 2.9 %slice-start = ((f32[512,512]{1,0:T(8,128)}), f32[1,512]{1,0:T(1,128)S(1)}, s32[]{:S(2)}) async-start(f32[512,512]{1,0:T(8,128)} %copy-done.1), calls=%async_computation.6 | async-start | bytes 4096 | tf_op jit(solution)/shard_map/slice | solution.py:99
  167.9 2.9 %copy-start.7 = (f32[255,512]{1,0:T(8,128)S(1)}, f32[255,512]{1,0:T(8,128)}, u32[]{:S(2)}) copy-start(f32[255,512]{1,0:T(8,128)} %get-tuple-element.130) | copy-start | bytes 1566724
  170.9 36.4 %copy-start.8 = (f32[512,512]{1,0:T(8,128)S(1)}, f32[512,512]{1,0:T(8,128)}, u32[]{:S(2)}) copy-start(f32[512,512]{1,0:T(8,128)} %pad.144) | copy-start | bytes 3145732
Sparse Core Ops, SparseCore 0:
  10.7 25.2 all-gather.5
  38.1 60.5 all-gather.7
  100.7 48.9 all-gather.9
  242.6 28.3 reduce-scatter.1
